TPU v7x, 32 devices: a whole 2x2x4 slice. The times are simulated.
32 devices in a mesh: rep: 2 (over x), fs: 8 (over z, y), tp: 2 (over core).
Axes of the slice: x: 2, y: 2, z: 4, core: 2. Of those that a mesh axis runs over, the one named last changes fastest.
Arguments:
- residual: bfloat16 [16, 384, 2048], P(('rep', 'fs'), None, 'tp'), may hold values from -6 to 6
- gain_first: float32 [2048], replicated, may hold values from 0.1 to 1.9
- gain_mixer: float32 [2048], replicated, may hold values from 0.1 to 1.9
- gain_last: float32 [2048], replicated, may hold values from 0.1 to 1.9
- hidden_gate: float32 [2048, 6144], P('fs', 'tp'), may hold values from -0.125 to 0.125
- hidden_up: float32 [2048, 6144], P('fs', 'tp'), may hold values from -0.125 to 0.125
- hidden_down: float32 [6144, 2048], P('tp', 'fs'), may hold values from -0.078125 to 0.078125
- gate_scale: float32 [6144], replicated, may hold values from 0.5 to 2
- up_scale: float32 [6144], replicated, may hold values from 0.5 to 2
- down_scale: float32 [2048], replicated, may hold values from 0.5 to 2
- mix_value: float32 [2048, 2048], P('fs', 'tp'), may hold values from -0.125 to 0.125
- mix_gate: float32 [2048, 2048], P('fs', 'tp'), may hold values from -0.125 to 0.125
- value_scale: float32 [2048], replicated, may hold values from 0.5 to 2
- gating_scale: float32 [2048], replicated, may hold values from 0.5 to 2
- mix_taps: float32 [31, 2048], replicated, may hold values from -1.25 to 1.25
- mix_gain: float32 [2048], replicated, may hold values from 0.1 to 1.9
- mix_out: float32 [2048, 2048], P('tp', 'fs'), may hold values from -0.125 to 0.125
- out_scale: float32 [2048], replicated, may hold values from 0.5 to 2
Outputs:
- updated: bfloat16 [16, 384, 2048], P(('rep', 'fs'), None, 'tp')
All inputs are finite; a program needn't handle non-finite values.
Results may differ from a plain program's by a relative error of at most 0.024.
Values may be sent and summed in bfloat16 or wider, within the bound.
A program may use at most 128 MiB of HBM per device.

v0:
```python
import jax
import jax.numpy as jnp
from jax import lax
from jax.sharding import PartitionSpec as P

EPS = 1e-06


def fold_rows(normed, pieces):
    return (
        jnp.dot(normed, pieces[0], preferred_element_type=jnp.float32),
        jnp.dot(normed, pieces[1], preferred_element_type=jnp.float32),
    )


def column_product(left, scale, piece):
    return jnp.dot(left, piece, preferred_element_type=jnp.float32) * scale


def on_device(
    residual,
    gain_first,
    gain_mixer,
    gain_last,
    hidden_gate,
    hidden_up,
    hidden_down,
    gate_scale,
    up_scale,
    down_scale,
    mix_value,
    mix_gate,
    value_scale,
    gating_scale,
    mix_taps,
    mix_gain,
    mix_out,
    out_scale,
):
    tp_rank = lax.axis_index("tp")
    hidden_local = hidden_gate.shape[1]
    width_local = residual.shape[2]
    seq_len = residual.shape[1]
    gate_cols = lax.dynamic_slice_in_dim(gate_scale, tp_rank * hidden_local, hidden_local)
    up_cols = lax.dynamic_slice_in_dim(up_scale, tp_rank * hidden_local, hidden_local)
    value_cols = lax.dynamic_slice_in_dim(value_scale, tp_rank * width_local, width_local)
    gating_cols = lax.dynamic_slice_in_dim(gating_scale, tp_rank * width_local, width_local)
    gain_cols = lax.dynamic_slice_in_dim(mix_gain, tp_rank * width_local, width_local)
    tap_cols = lax.dynamic_slice_in_dim(mix_taps, tp_rank * width_local, width_local, 1)
    gate_half = hidden_gate.astype(jnp.bfloat16)
    up_half = hidden_up.astype(jnp.bfloat16)
    down_half = hidden_down.astype(jnp.bfloat16)
    value_half = mix_value.astype(jnp.bfloat16)
    mgate_half = mix_gate.astype(jnp.bfloat16)
    out_half = mix_out.astype(jnp.bfloat16)

    def normed_rows(stream, gain):
        gathered = lax.all_gather(stream, "tp", axis=1, tiled=True)
        values = gathered.astype(jnp.float32)
        scaled = values * lax.rsqrt(jnp.mean(values * values, axis=-1, keepdims=True) + EPS) * gain
        return scaled.astype(jnp.bfloat16)

    def spread_sum(terms):
        return lax.psum_scatter(
            terms.astype(jnp.bfloat16), "tp", scatter_dimension=1, tiled=True
        ).astype(jnp.float32)

    def inner_half(stream, gain):
        normed = normed_rows(stream, gain)
        gate, upward = fold_rows(
            normed,
            (
                lax.all_gather(gate_half, "fs", axis=0, tiled=True),
                lax.all_gather(up_half, "fs", axis=0, tiled=True),
            ),
        )
        hidden = (jax.nn.silu(gate * gate_cols) * (upward * up_cols)).astype(jnp.bfloat16)
        terms = column_product(
            hidden, down_scale, lax.all_gather(down_half, "fs", axis=1, tiled=True)
        )
        return spread_sum(terms)

    stream = residual[0]
    first = (stream.astype(jnp.float32) + 0.5 * inner_half(stream, gain_first)).astype(jnp.bfloat16)
    normed = normed_rows(first, gain_mixer)
    value, gating = fold_rows(
        normed,
        (
            lax.all_gather(value_half, "fs", axis=0, tiled=True),
            lax.all_gather(mgate_half, "fs", axis=0, tiled=True),
        ),
    )
    glu = lax.optimization_barrier(
        (value * value_cols * jax.nn.sigmoid(gating * gating_cols)).astype(jnp.bfloat16)
    ).astype(jnp.float32)
    span = tap_cols.shape[0]
    padded = jnp.pad(glu, ((span - 1, 0), (0, 0)))
    wave = jnp.zeros_like(glu)
    for offset in range(span):
        wave = wave + tap_cols[offset] * padded[span - 1 - offset : span - 1 - offset + seq_len]
    total_sq = lax.psum(jnp.sum(wave * wave, axis=1), "tp")
    inverse = lax.rsqrt(total_sq / mix_taps.shape[1] + EPS)
    acted = jax.nn.silu(wave * inverse[:, None] * gain_cols).astype(jnp.bfloat16)
    terms = column_product(acted, out_scale, lax.all_gather(out_half, "fs", axis=1, tiled=True))
    second = (first.astype(jnp.float32) + spread_sum(terms)).astype(jnp.bfloat16)
    updated = (second.astype(jnp.float32) + 0.5 * inner_half(second, gain_last)).astype(
        jnp.bfloat16
    )
    return updated[None]


def solution(mesh):
    in_specs = (
        P(("rep", "fs"), None, "tp"),
        P(),
        P(),
        P(),
        P("fs", "tp"),
        P("fs", "tp"),
        P("tp", "fs"),
        P(),
        P(),
        P(),
        P("fs", "tp"),
        P("fs", "tp"),
        P(),
        P(),
        P(),
        P(),
        P("tp", "fs"),
        P(),
    )
    out_specs = P(("rep", "fs"), None, "tp")
    return jax.shard_map(
        on_device, mesh=mesh, in_specs=in_specs, out_specs=out_specs, check_vma=False
    )
```

profile of v0, /device:TPU:0, one launch (start us, length us, event | category | flops | bytes accessed | tf_op | source)
XLA Modules:
  0.0 900.1 jit_solution(637089719911600828)
XLA Ops:
  6.5 0.7 all-gather.27.cloned.1.call-update
  7.3 3.4 convert_element_type.92
  10.7 0.0 all-gather.13.cloned.1.call-start
  10.8 1.4 convert_element_type.93
  12.3 0.0 all-gather.15.cloned.1.call-start
  12.3 3.2 convert_element_type.95
  15.5 0.0 reduce-scatter.4.cloned.1.call-start
  15.6 0.7 copy-done.10
  16.3 5.2 all-gather.27.cloned.1.call-done
  21.4 1.9 fusion.6
  23.4 177.6 %all-gather.11.cloned.1.call-done = bf16[2048,3072]{1,0:T(8,128)(2,1)} async-done(((bf16[256,3072]{1,0:T(8,128)(2,1)}), bf16[2048,3072]{1,0:T(8,128)(2,1)}) %all-gather.11.cloned.1.call-update) | async-done | bytes 12582928 | tf_op jit(solution)/shard_map/all_gather | solution.py:73
  200.9 10.3 %fusion.22 = f32[384,3072]{1,0:T(8,128)} fusion(bf16[2048,3072]{1,0:T(8,128)(2,1)} %all-gather.11.cloned.1.call-done, bf16[1,384,2048]{2,1,0:T(8,128)(2,1)S(1)} %copy-done.5, f32[2048]{0:T(1024)S(1)} %copy-done.12, f32[384]{0:T(512)S(1)} %add_rsqrt_fusion.3), kind=kOutput, calls=%fused_computation.41 | convolution fusion | flops 4834983936 | bytes 18884096 | tf_op jit(solution)/shard_map/dot_general | solution.py:11
  211.3 166.2 %all-gather.13.cloned.1.call-done = bf16[2048,3072]{1,0:T(8,128)(2,1)} async-done(((bf16[256,3072]{1,0:T(8,128)(2,1)}), bf16[2048,3072]{1,0:T(8,128)(2,1)}) %all-gather.13.cloned.1.call-update) | async-done | bytes 12582928 | tf_op jit(solution)/shard_map/all_gather | solution.py:74
  377.4 176.2 %all-gather.15.cloned.1.call-done = bf16[3072,2048]{1,0:T(8,128)(2,1)} async-done(((bf16[3072,256]{1,0:T(8,128)(2,1)}), bf16[3072,2048]{1,0:T(8,128)(2,1)}) %all-gather.15.cloned.1.call-update) | async-done | bytes 12582928 | tf_op jit(solution)/shard_map/all_gather | solution.py:79
  553.7 21.3 %multiply_convert_fusion.4 = bf16[384,2048]{1,0:T(8,128)(2,1)} fusion(bf16[3072,2048]{1,0:T(8,128)(2,1)} %all-gather.15.cloned.1.call-done, f32[2048]{0:T(1024)S(1)} %copy-done.15, f32[384,3072]{1,0:T(8,128)} %fusion.22, bf16[2048,3072]{1,0:T(8,128)(2,1)} %all-gather.13.cloned.1.call-done, f32[3072]{0:T(1024)S(1)} %dynamic_slice.19, ...), kind=kOutput, calls=%fused_computation.19 | convolution fusion | flops 9677832192 | bytes 33072640 | tf_op jit(solution)/shard_map/dot_general | solution.py:17
  575.0 0.0 all-gather.17.cloned.1.call-start
  575.1 7.2 reduce-scatter.4.cloned.1.call-done
  582.3 2.3 fusion.9
  584.6 0.0 all-gather.19.cloned.1.call-start
  584.7 0.9 convert_element_type.102
  585.6 0.2 all-gather.21.cloned.1.call-start
  585.8 0.2 copy-done.8
  586.0 0.9 convert_element_type.103
  586.9 0.0 all-gather.23.cloned.1.call-start
  586.9 0.9 convert_element_type.107
  587.8 0.0 reduce-scatter.6.cloned.1.call-start
  587.9 1.3 fusion.34
  589.2 1.6 constant_dynamic-slice_fusion
  590.8 5.1 all-gather.17.cloned.1.call-done
  595.8 1.9 fusion
  597.8 74.2 %all-gather.19.cloned.1.call-done = bf16[2048,1024]{1,0:T(8,128)(2,1)} async-done(((bf16[256,1024]{1,0:T(8,128)(2,1)}), bf16[2048,1024]{1,0:T(8,128)(2,1)}) %all-gather.19.cloned.1.call-update) | async-done | bytes 4194320 | tf_op jit(solution)/shard_map/all_gather | solution.py:89
  672.0 5.2 fusion.29
  677.2 68.3 %all-gather.21.cloned.1.call-done = bf16[2048,1024]{1,0:T(8,128)(2,1)} async-done(((bf16[256,1024]{1,0:T(8,128)(2,1)}), bf16[2048,1024]{1,0:T(8,128)(2,1)}) %all-gather.21.cloned.1.call-update) | async-done | bytes 4194320 | tf_op jit(solution)/shard_map/all_gather | solution.py:90
  745.4 4.7 multiply_convert_fusion.6
  750.2 0.2 convert_element_type.105
  750.4 7.3 multiply_reduce_fusion
  757.7 2.5 psum.7
  760.1 60.6 %all-gather.23.cloned.1.call-done = bf16[1024,2048]{1,0:T(8,128)(2,1)} async-done(((bf16[1024,256]{1,0:T(8,128)(2,1)}), bf16[1024,2048]{1,0:T(8,128)(2,1)}) %all-gather.23.cloned.1.call-update) | async-done | bytes 4194320 | tf_op jit(solution)/shard_map/all_gather | solution.py:104
  820.7 5.5 multiply_convert_fusion.3
  826.3 7.2 reduce-scatter.6.cloned.1.call-done
  833.5 2.3 add_convert_fusion.1
  835.9 0.3 reduce-scatter.8.cloned.1.call-start
  836.1 11.0 %all-gather.25.cloned.1.call-done = bf16[384,2048]{1,0:T(8,128)(2,1)} async-done(((bf16[384,1024]{1,0:T(8,128)(2,1)}), bf16[384,2048]{1,0:T(8,128)(2,1)}) %all-gather.25.cloned.1.call-update) | async-done | bytes 1572880 | tf_op jit(solution)/shard_map/all_gather | solution.py:58
  847.1 1.9 fusion.3
  849.0 10.3 %fusion.26 = f32[384,3072]{1,0:T(8,128)} fusion(bf16[2048,3072]{1,0:T(8,128)(2,1)} %all-gather.11.cloned.1.call-done, bf16[384,2048]{1,0:T(8,128)(2,1)S(1)} %copy-done.6, f32[2048]{0:T(1024)S(1)} %copy-done.16, f32[384]{0:T(512)S(1)} %add_rsqrt_fusion), kind=kOutput, calls=%fused_computation.42 | convolution fusion | flops 4834983936 | bytes 18884096 | tf_op jit(solution)/shard_map/dot_general | solution.py:11
  859.3 21.3 %multiply_convert_fusion.2 = bf16[384,2048]{1,0:T(8,128)(2,1)} fusion(bf16[3072,2048]{1,0:T(8,128)(2,1)} %all-gather.15.cloned.1.call-done, f32[2048]{0:T(1024)S(1)} %copy-done.15, f32[384,3072]{1,0:T(8,128)} %fusion.26, bf16[2048,3072]{1,0:T(8,128)(2,1)} %all-gather.13.cloned.1.call-done, f32[3072]{0:T(1024)S(1)} %dynamic_slice.19, ...), kind=kOutput, calls=%fused_computation.17 | convolution fusion | flops 9677832192 | bytes 33072640 | tf_op jit(solution)/shard_map/dot_general | solution.py:17
  880.6 10.3 %reduce-scatter.8.cloned.1.call-done = bf16[384,1024]{1,0:T(8,128)(2,1)} async-done(((bf16[384,2048]{1,0:T(8,128)(2,1)}), bf16[384,1024]{1,0:T(8,128)(2,1)}) %reduce-scatter.8.cloned.1.call-update) | async-done | bytes 786448 | tf_op jit(solution)/shard_map/reduce_scatter | solution.py:64
  890.9 2.3 fusion.16
  (58 shorter events, 0.4 us)
Async XLA Ops:
  6.5 14.9 %all-gather.27.cloned.1.call-start = ((), (), s32[]{:S(2)}) async-start(), calls=%async_computation.14 | async-start | bytes 2359296 | tf_op jit(solution)/shard_map/all_gather | solution.py:58
  7.3 193.7 %all-gather.11.cloned.1.call-start = ((), (), s32[]{:S(2)}) async-start(), calls=%async_computation.3 | async-start | bytes 14155776 | tf_op jit(solution)/shard_map/all_gather | solution.py:73
  7.3 3.5 copy-start.2
  10.7 366.7 %all-gather.13.cloned.1.call-start = ((), (), s32[]{:S(2)}) async-start(), calls=%async_computation.4 | async-start | bytes 14155776 | tf_op jit(solution)/shard_map/all_gather | solution.py:74
  12.3 541.4 %all-gather.15.cloned.1.call-start = ((), (), s32[]{:S(2)}) async-start(), calls=%async_computation.5 | async-start | bytes 14155776 | tf_op jit(solution)/shard_map/all_gather | solution.py:79
  15.5 0.7 copy-start.10
  15.5 0.8 copy-start.11
  15.5 185.4 %copy-start.12 = (f32[2048]{0:T(1024)S(1)}, f32[2048]{0:T(1024)}, u32[]{:S(2)}) copy-start(f32[2048]{0:T(1024)} %param.19) | copy-start | bytes 24580
  15.5 566.7 %reduce-scatter.4.cloned.1.call-start = ((), (), s32[]{:S(2)}) async-start(), calls=%async_computation.6 | async-start | bytes 2359296 | tf_op jit(solution)/shard_map/reduce_scatter | solution.py:64
  21.4 179.5 %copy-start.5 = (bf16[1,384,2048]{2,1,0:T(8,128)(2,1)S(1)}, bf16[1,384,2048]{2,1,0:T(8,128)(2,1)}, u32[]{:S(2)}) copy-start(bf16[1,384,2048]{2,1,0:T(8,128)(2,1)} %all-gather.27.cloned.1.call-done) | copy-start | bytes 4718596
  23.4 530.3 %copy-start.15 = (f32[2048]{0:T(1024)S(1)}, f32[2048]{0:T(1024)}, u32[]{:S(2)}) copy-start(f32[2048]{0:T(1024)} %param.27) | copy-start | bytes 24580
  575.0 7.3 copy-start.3
  575.0 9.7 %copy-start.7 = (f32[256,1024]{1,0:T(8,128)S(1)}, f32[256,1024]{1,0:T(8,128)}, u32[]{:S(2)}) copy-start(f32[256,1024]{1,0:T(8,128)} %param.28) | copy-start | bytes 3145732
  575.0 20.8 %all-gather.17.cloned.1.call-start = ((), (), s32[]{:S(2)}) async-start(), calls=%async_computation.7 | async-start | bytes 2359296 | tf_op jit(solution)/shard_map/all_gather | solution.py:58
  584.6 1.4 copy-start.8
  584.6 87.4 %all-gather.19.cloned.1.call-start = ((), (), s32[]{:S(2)}) async-start(), calls=%async_computation.8 | async-start | bytes 4718592 | tf_op jit(solution)/shard_map/all_gather | solution.py:89
  585.5 1.4 copy-start.9
  585.6 159.9 %all-gather.21.cloned.1.call-start = ((), (), s32[]{:S(2)}) async-start(), calls=%async_computation.9 | async-start | bytes 4718592 | tf_op jit(solution)/shard_map/all_gather | solution.py:90
  586.9 233.8 %all-gather.23.cloned.1.call-start = ((), (), s32[]{:S(2)}) async-start(), calls=%async_computation.10 | async-start | bytes 4718592 | tf_op jit(solution)/shard_map/all_gather | solution.py:104
  587.8 84.2 %copy-start.13 = (f32[2048]{0:T(1024)S(1)}, f32[2048]{0:T(1024)}, u32[]{:S(2)}) copy-start(f32[2048]{0:T(1024)} %param.20) | copy-start | bytes 24580
  587.8 245.7 %reduce-scatter.6.cloned.1.call-start = ((), (), s32[]{:S(2)}) async-start(), calls=%async_computation.11 | async-start | bytes 2359296 | tf_op jit(solution)/shard_map/reduce_scatter | solution.py:64
  595.8 76.1 %copy-start.4 = (bf16[384,2048]{1,0:T(8,128)(2,1)S(1)}, bf16[384,2048]{1,0:T(8,128)(2,1)}, u32[]{:S(2)}) copy-start(bf16[384,2048]{1,0:T(8,128)(2,1)} %all-gather.17.cloned.1.call-done) | copy-start | bytes 4718596
  597.8 147.7 %dynamic-slice-start = ((f32[2048]{0:T(1024)}, s32[]{:T(128)}), f32[1024]{0:T(1024)S(1)}, s32[]{:S(2)}) async-start(f32[2048]{0:T(1024)} %param.30, s32[]{:T(128)} %select_n.5), calls=%async_computation.15 | async-start | bytes 8704 | tf_op jit(solution)/shard_map/dynamic_slice | solution.py:46
  597.8 147.7 %dynamic-slice-start.1 = ((f32[2048]{0:T(1024)}, s32[]{:T(128)}), f32[1024]{0:T(1024)S(1)}, s32[]{:S(2)}) async-start(f32[2048]{0:T(1024)} %param.31, s32[]{:T(128)} %select_n.5), calls=%async_computation.16 | async-start | bytes 8704 | tf_op jit(solution)/shard_map/dynamic_slice | solution.py:47
  750.4 70.3 %dynamic-slice-start.2 = ((f32[2048]{0:T(1024)}, s32[]{:T(128)}), f32[1024]{0:T(1024)S(1)}, s32[]{:S(2)}) async-start(f32[2048]{0:T(1024)} %param.33, s32[]{:T(128)} %select_n.5), calls=%async_computation.17 | async-start | bytes 8704 | tf_op jit(solution)/shard_map/dynamic_slice | solution.py:48
  750.4 70.3 %copy-start.14 = (f32[2048]{0:T(1024)S(1)}, f32[2048]{0:T(1024)}, u32[]{:S(2)}) copy-start(f32[2048]{0:T(1024)} %param.35) | copy-start | bytes 24580
  826.2 7.3 copy-start
  826.2 20.9 %all-gather.25.cloned.1.call-start = ((), (), s32[]{:S(2)}) async-start(), calls=%async_computation.12 | async-start | bytes 2359296 | tf_op jit(solution)/shard_map/all_gather | solution.py:58
  835.8 13.2 %copy-start.16 = (f32[2048]{0:T(1024)S(1)}, f32[2048]{0:T(1024)}, u32[]{:S(2)}) copy-start(f32[2048]{0:T(1024)} %param.21) | copy-start | bytes 24580
  835.9 55.0 %reduce-scatter.8.cloned.1.call-start = ((), (), s32[]{:S(2)}) async-start(), calls=%async_computation.13 | async-start | bytes 2359296 | tf_op jit(solution)/shard_map/reduce_scatter | solution.py:64
  847.1 1.9 copy-start.6
  880.6 10.3 %copy-start.1 = (bf16[384,1024]{1,0:T(8,128)(2,1)S(1)}, bf16[384,1024]{1,0:T(8,128)(2,1)}, u32[]{:S(2)}) copy-start(bf16[384,1024]{1,0:T(8,128)(2,1)} %add_convert_fusion.1) | copy-start | bytes 2359300
Sparse Core Ops, SparseCore 0:
  8.9 12.5 all-gather.26
  23.6 177.2 all-gather.10
  203.1 174.2 all-gather.12
  379.3 174.2 all-gather.14
  575.1 7.0 reduce-scatter.3
  584.7 11.0 all-gather.16
  598.0 73.9 all-gather.18
  674.1 71.3 all-gather.20
  747.5 73.1 all-gather.22
  826.3 7.1 reduce-scatter.5
  836.0 11.0 all-gather.24
  880.7 10.1 reduce-scatter.7
where the time goes:
time: 901 us; the launch traced here: 900 us
  waiting for transfers between devices  770 us (85%)
  matrix products  78.6 us (9%)
  other arithmetic  30.8 us (3%)
  between operations  13.7 us (2%)
    all_gather x1, waiting for transfers between devices, inner_half(): lax.all_gather(gate_half, 'fs', axis=0, tiled=True)  178 us
    all_gather x1, waiting for transfers between devices, inner_half(): lax.all_gather(down_half, 'fs', axis=1, tiled=True)  176 us
    all_gather x1, waiting for transfers between devices, inner_half(): lax.all_gather(up_half, 'fs', axis=0, tiled=True)  166 us
    all_gather x1, waiting for transfers between devices, on_device(): lax.all_gather(value_half, 'fs', axis=0, tiled=True)  74.2 us
    all_gather x1, waiting for transfers between devices, on_device(): lax.all_gather(mgate_half, 'fs', axis=0, tiled=True)  68.3 us
    all_gather x1, waiting for transfers between devices, on_device(): lax.all_gather(out_half, 'fs', axis=1, tiled=True)  60.6 us
    dot_general x3, matrix products, column_product(): return jnp.dot(left, piece, preferred_element_type=jnp.float32) * scale  48.1 us
    dot_general x3, matrix products, fold_rows(): jnp.dot(normed, pieces[0], preferred_element_type=jnp.float32)  25.9 us
  transfers between devices with their start and end apart: 12, of which 12 were waited for; matrix products, arithmetic and copies ran while one was open for 5% of the time, Pallas kernels for 0%

commit v1 on v0

--- a/solution.py
+++ b/solution.py
@@ -4,6 +4,12 @@
 from jax.sharding import PartitionSpec as P
 
 EPS = 1e-06
+
+
+def gathered_along(block, axis, dim):
+    shards = lax.all_gather(block, axis, axis=0, tiled=False)
+    result = jnp.concatenate(shards, axis=dim)
+    return result
 
 
 def fold_rows(normed, pieces):
@@ -75,9 +81,7 @@
             ),
         )
         hidden = (jax.nn.silu(gate * gate_cols) * (upward * up_cols)).astype(jnp.bfloat16)
-        terms = column_product(
-            hidden, down_scale, lax.all_gather(down_half, "fs", axis=1, tiled=True)
-        )
+        terms = column_product(hidden, down_scale, gathered_along(down_half, "fs", 1))
         return spread_sum(terms)
 
     stream = residual[0]

time: 901 us -> 892 us (0.990)
  waiting for transfers between devices: 770 us -> 753 us
  local copies, waits for them, and re-layouts: 3.84 us -> 20.7 us
  matrix products: 78.6 us -> 69.3 us
    all_gather x1, waiting for transfers between devices: 178 us -> 160 us  [inner_half(): lax.all_gather(gate_half, 'fs', axis=0, tiled=True)]
    reshape x0 -> x1, local copies, waits for them, and re-layouts: none -> 16.7 us  [gathered_along(): result = jnp.concatenate(shards, axis=dim)]
    dot_general x3, matrix products: 48.1 us -> 38.7 us  [column_product(): return jnp.dot(left, piece, preferred_element_type=jnp.float32) * scale]
  transfers between devices with their start and end apart: 12 -> 12, of which waited for: 12 -> 12; matrix products, arithmetic and copies ran while one was open for 5% -> 7% of each run, Pallas kernels for 0% -> 0%
where the time goes in v1:
time: 892 us; the launch traced here: 891 us
  waiting for transfers between devices  753 us (84%)
  matrix products  69.3 us (8%)
  other arithmetic  30.6 us (3%)
  local copies, waits for them, and re-layouts  20.7 us (2%)
  between operations  13.7 us (2%)
    all_gather x1, waiting for transfers between devices, gathered_along(): shards = lax.all_gather(block, axis, axis=0, tiled=False)  178 us
    all_gather x1, waiting for transfers between devices, inner_half(): lax.all_gather(up_half, 'fs', axis=0, tiled=True)  166 us
    all_gather x1, waiting for transfers between devices, inner_half(): lax.all_gather(gate_half, 'fs', axis=0, tiled=True)  160 us
    all_gather x1, waiting for transfers between devices, on_device(): lax.all_gather(value_half, 'fs', axis=0, tiled=True)  74.2 us
    all_gather x1, waiting for transfers between devices, on_device(): lax.all_gather(mgate_half, 'fs', axis=0, tiled=True)  68.3 us
    all_gather x1, waiting for transfers between devices, on_device(): lax.all_gather(out_half, 'fs', axis=1, tiled=True)  60.6 us
    dot_general x3, matrix products, column_product(): return jnp.dot(left, piece, preferred_element_type=jnp.float32) * scale  38.7 us
    dot_general x3, matrix products, fold_rows(): jnp.dot(normed, pieces[0], preferred_element_type=jnp.float32)  25.8 us
  transfers between devices with their start and end apart: 12, of which 12 were waited for; matrix products, arithmetic and copies ran while one was open for 7% of the time, Pallas kernels for 0%

profile of v1, /device:TPU:0, one launch (start us, length us, event | category | flops | bytes accessed | tf_op | source)
XLA Modules:
  0.0 890.9 jit_solution(9603984996028929789)
XLA Ops:
  6.5 0.7 all-gather.26.cloned.1.call-update
  7.3 3.4 convert_element_type.95
  10.7 0.0 all-gather.12.cloned.1.call-start
  10.8 1.4 convert_element_type.92
  12.1 0.0 all-gather.14.cloned.1.call-start
  12.2 3.3 convert_element_type.93
  15.5 0.0 reduce-scatter.4.cloned.1.call-start
  15.5 0.7 copy-done.10
  16.2 5.2 all-gather.26.cloned.1.call-done
  21.4 1.8 fusion.6
  23.2 177.7 %all-gather.28.cloned.1.call-done = bf16[24576,256]{1,0:T(8,128)(2,1)} async-done(((bf16[3072,256]{1,0:T(8,128)(2,1)}), bf16[24576,256]{1,0:T(8,128)(2,1)}) %all-gather.28.cloned.1.call-update) | async-done | bytes 12582928 | tf_op jit(solution)/shard_map/all_gather | solution.py:10
  200.9 16.7 %copy.19 = bf16[3072,8,256]{0,2,1:T(8,128)(2,1)} copy(bf16[3072,8,256]{2,0,1:T(8,128)(2,1)} %bitcast.58) | data formatting | bytes 25165824 | tf_op jit(solution)/shard_map/reshape | solution.py:11
  217.6 159.8 %all-gather.12.cloned.1.call-done = bf16[2048,3072]{1,0:T(8,128)(2,1)} async-done(((bf16[256,3072]{1,0:T(8,128)(2,1)}), bf16[2048,3072]{1,0:T(8,128)(2,1)}) %all-gather.12.cloned.1.call-update) | async-done | bytes 12582928 | tf_op jit(solution)/shard_map/all_gather | solution.py:79
  377.4 10.3 %fusion.22 = f32[384,3072]{1,0:T(8,128)} fusion(bf16[2048,3072]{1,0:T(8,128)(2,1)} %all-gather.12.cloned.1.call-done, bf16[1,384,2048]{2,1,0:T(8,128)(2,1)S(1)} %copy-done.5, f32[2048]{0:T(1024)S(1)} %copy-done.12, f32[384]{0:T(512)S(1)} %add_rsqrt_fusion.3), kind=kOutput, calls=%fused_computation.41 | convolution fusion | flops 4834983936 | bytes 18884096 | tf_op jit(solution)/shard_map/dot_general | solution.py:17
  387.8 166.0 %all-gather.14.cloned.1.call-done = bf16[2048,3072]{1,0:T(8,128)(2,1)} async-done(((bf16[256,3072]{1,0:T(8,128)(2,1)}), bf16[2048,3072]{1,0:T(8,128)(2,1)}) %all-gather.14.cloned.1.call-update) | async-done | bytes 12582928 | tf_op jit(solution)/shard_map/all_gather | solution.py:80
  553.8 16.6 %multiply_convert_fusion.4 = bf16[384,2048]{1,0:T(8,128)(2,1)} fusion(bf16[3072,2048]{0,1:T(8,128)(2,1)} %bitcast.56, f32[2048]{0:T(1024)S(1)} %copy-done.15, f32[384,3072]{1,0:T(8,128)} %fusion.22, bf16[2048,3072]{1,0:T(8,128)(2,1)} %all-gather.14.cloned.1.call-done, f32[3072]{0:T(1024)S(1)} %dynamic_slice.19, f32[3072]{0:T(1024)S(1)} %dynamic_slice.18, ...), kind=kOutput, calls=%fused_computation.19 | convolution fusion | flops 9677832192 | bytes 33072640 | tf_op jit(solution)/shard_map/dot_general | solution.py:23
  570.5 0.0 all-gather.16.cloned.1.call-start
  570.5 7.2 reduce-scatter.4.cloned.1.call-done
  577.7 2.3 fusion.9
  580.1 0.9 convert_element_type.102
  581.1 0.4 copy-done.8
  581.5 0.9 convert_element_type.103
  582.3 0.0 all-gather.22.cloned.1.call-start
  582.4 0.9 convert_element_type.107
  583.3 0.2 reduce-scatter.6.cloned.1.call-start
  583.5 1.3 fusion.34
  584.8 1.6 constant_dynamic-slice_fusion
  586.4 4.9 all-gather.16.cloned.1.call-done
  591.3 1.9 fusion
  593.2 74.2 %all-gather.18.cloned.1.call-done = bf16[2048,1024]{1,0:T(8,128)(2,1)} async-done(((bf16[256,1024]{1,0:T(8,128)(2,1)}), bf16[2048,1024]{1,0:T(8,128)(2,1)}) %all-gather.18.cloned.1.call-update) | async-done | bytes 4194320 | tf_op jit(solution)/shard_map/all_gather | solution.py:93
  667.4 5.2 fusion.29
  672.6 68.3 %all-gather.20.cloned.1.call-done = bf16[2048,1024]{1,0:T(8,128)(2,1)} async-done(((bf16[256,1024]{1,0:T(8,128)(2,1)}), bf16[2048,1024]{1,0:T(8,128)(2,1)}) %all-gather.20.cloned.1.call-update) | async-done | bytes 4194320 | tf_op jit(solution)/shard_map/all_gather | solution.py:94
  740.9 4.7 multiply_convert_fusion.6
  745.6 0.2 convert_element_type.105
  745.9 7.3 multiply_reduce_fusion
  753.1 2.5 psum.7
  755.6 60.6 %all-gather.22.cloned.1.call-done = bf16[1024,2048]{1,0:T(8,128)(2,1)} async-done(((bf16[1024,256]{1,0:T(8,128)(2,1)}), bf16[1024,2048]{1,0:T(8,128)(2,1)}) %all-gather.22.cloned.1.call-update) | async-done | bytes 4194320 | tf_op jit(solution)/shard_map/all_gather | solution.py:108
  816.2 5.5 multiply_convert_fusion.3
  821.7 0.0 all-gather.24.cloned.1.call-start
  821.7 7.2 reduce-scatter.6.cloned.1.call-done
  829.0 2.3 add_convert_fusion.1
  831.3 0.3 reduce-scatter.8.cloned.1.call-start
  831.6 11.0 %all-gather.24.cloned.1.call-done = bf16[384,2048]{1,0:T(8,128)(2,1)} async-done(((bf16[384,1024]{1,0:T(8,128)(2,1)}), bf16[384,2048]{1,0:T(8,128)(2,1)}) %all-gather.24.cloned.1.call-update) | async-done | bytes 1572880 | tf_op jit(solution)/shard_map/all_gather | solution.py:64
  842.5 1.9 fusion.3
  844.5 10.3 %fusion.26 = f32[384,3072]{1,0:T(8,128)} fusion(bf16[2048,3072]{1,0:T(8,128)(2,1)} %all-gather.12.cloned.1.call-done, bf16[384,2048]{1,0:T(8,128)(2,1)S(1)} %copy-done.6, f32[2048]{0:T(1024)S(1)} %copy-done.16, f32[384]{0:T(512)S(1)} %add_rsqrt_fusion), kind=kOutput, calls=%fused_computation.42 | convolution fusion | flops 4834983936 | bytes 18884096 | tf_op jit(solution)/shard_map/dot_general | solution.py:17
  854.8 16.6 %multiply_convert_fusion.2 = bf16[384,2048]{1,0:T(8,128)(2,1)} fusion(bf16[3072,2048]{0,1:T(8,128)(2,1)} %bitcast.57, f32[2048]{0:T(1024)S(1)} %copy-done.15, f32[384,3072]{1,0:T(8,128)} %fusion.26, bf16[2048,3072]{1,0:T(8,128)(2,1)} %all-gather.14.cloned.1.call-done, f32[3072]{0:T(1024)S(1)} %dynamic_slice.19, f32[3072]{0:T(1024)S(1)} %dynamic_slice.18, ...), kind=kOutput, calls=%fused_computation.17 | convolution fusion | flops 9677832192 | bytes 33072640 | tf_op jit(solution)/shard_map/dot_general | solution.py:23
  871.4 10.3 %reduce-scatter.8.cloned.1.call-done = bf16[384,1024]{1,0:T(8,128)(2,1)} async-done(((bf16[384,2048]{1,0:T(8,128)(2,1)}), bf16[384,1024]{1,0:T(8,128)(2,1)}) %reduce-scatter.8.cloned.1.call-update) | async-done | bytes 786448 | tf_op jit(solution)/shard_map/reduce_scatter | solution.py:70
  881.7 2.3 fusion.16
  (59 shorter events, 0.4 us)
Async XLA Ops:
  6.5 14.9 %all-gather.26.cloned.1.call-start = ((), (), s32[]{:S(2)}) async-start(), calls=%async_computation.13 | async-start | bytes 2359296 | tf_op jit(solution)/shard_map/all_gather | solution.py:64
  7.3 193.7 %all-gather.28.cloned.1.call-start = ((), (), s32[]{:S(2)}) async-start(), calls=%async_computation.14 | async-start | bytes 14155776 | tf_op jit(solution)/shard_map/all_gather | solution.py:10
  7.3 3.5 copy-start.2
  10.7 366.7 %all-gather.12.cloned.1.call-start = ((), (), s32[]{:S(2)}) async-start(), calls=%async_computation.3 | async-start | bytes 14155776 | tf_op jit(solution)/shard_map/all_gather | solution.py:79
  12.1 541.7 %all-gather.14.cloned.1.call-start = ((), (), s32[]{:S(2)}) async-start(), calls=%async_computation.4 | async-start | bytes 14155776 | tf_op jit(solution)/shard_map/all_gather | solution.py:80
  15.5 0.7 copy-start.10
  15.5 0.8 copy-start.11
  15.5 562.2 %reduce-scatter.4.cloned.1.call-start = ((), (), s32[]{:S(2)}) async-start(), calls=%async_computation.5 | async-start | bytes 2359296 | tf_op jit(solution)/shard_map/reduce_scatter | solution.py:70
  200.9 176.5 %copy-start.5 = (bf16[1,384,2048]{2,1,0:T(8,128)(2,1)S(1)}, bf16[1,384,2048]{2,1,0:T(8,128)(2,1)}, u32[]{:S(2)}) copy-start(bf16[1,384,2048]{2,1,0:T(8,128)(2,1)} %all-gather.26.cloned.1.call-done) | copy-start | bytes 4718596
  200.9 176.5 %copy-start.12 = (f32[2048]{0:T(1024)S(1)}, f32[2048]{0:T(1024)}, u32[]{:S(2)}) copy-start(f32[2048]{0:T(1024)} %param.19) | copy-start | bytes 24580
  217.6 336.2 %copy-start.15 = (f32[2048]{0:T(1024)S(1)}, f32[2048]{0:T(1024)}, u32[]{:S(2)}) copy-start(f32[2048]{0:T(1024)} %param.27) | copy-start | bytes 24580
  570.4 7.3 copy-start.3
  570.4 9.7 %copy-start.7 = (f32[256,1024]{1,0:T(8,128)S(1)}, f32[256,1024]{1,0:T(8,128)}, u32[]{:S(2)}) copy-start(f32[256,1024]{1,0:T(8,128)} %param.28) | copy-start | bytes 3145732
  570.5 20.8 %all-gather.16.cloned.1.call-start = ((), (), s32[]{:S(2)}) async-start(), calls=%async_computation.6 | async-start | bytes 2359296 | tf_op jit(solution)/shard_map/all_gather | solution.py:64
  580.0 1.4 copy-start.8
  580.1 87.4 %all-gather.18.cloned.1.call-start = ((), (), s32[]{:S(2)}) async-start(), calls=%async_computation.7 | async-start | bytes 4718592 | tf_op jit(solution)/shard_map/all_gather | solution.py:93
  581.0 1.4 copy-start.9
  581.0 159.9 %all-gather.20.cloned.1.call-start = ((), (), s32[]{:S(2)}) async-start(), calls=%async_computation.8 | async-start | bytes 4718592 | tf_op jit(solution)/shard_map/all_gather | solution.py:94
  582.3 233.8 %all-gather.22.cloned.1.call-start = ((), (), s32[]{:S(2)}) async-start(), calls=%async_computation.9 | async-start | bytes 4718592 | tf_op jit(solution)/shard_map/all_gather | solution.py:108
  583.3 84.2 %copy-start.13 = (f32[2048]{0:T(1024)S(1)}, f32[2048]{0:T(1024)}, u32[]{:S(2)}) copy-start(f32[2048]{0:T(1024)} %param.20) | copy-start | bytes 24580
  583.3 245.7 %reduce-scatter.6.cloned.1.call-start = ((), (), s32[]{:S(2)}) async-start(), calls=%async_computation.10 | async-start | bytes 2359296 | tf_op jit(solution)/shard_map/reduce_scatter | solution.py:70
  591.3 76.1 %copy-start.4 = (bf16[384,2048]{1,0:T(8,128)(2,1)S(1)}, bf16[384,2048]{1,0:T(8,128)(2,1)}, u32[]{:S(2)}) copy-start(bf16[384,2048]{1,0:T(8,128)(2,1)} %all-gather.16.cloned.1.call-done) | copy-start | bytes 4718596
  593.2 147.7 %dynamic-slice-start = ((f32[2048]{0:T(1024)}, s32[]{:T(128)}), f32[1024]{0:T(1024)S(1)}, s32[]{:S(2)}) async-start(f32[2048]{0:T(1024)} %param.30, s32[]{:T(128)} %select_n.5), calls=%async_computation.15 | async-start | bytes 8704 | tf_op jit(solution)/shard_map/dynamic_slice | solution.py:52
  593.2 147.7 %dynamic-slice-start.1 = ((f32[2048]{0:T(1024)}, s32[]{:T(128)}), f32[1024]{0:T(1024)S(1)}, s32[]{:S(2)}) async-start(f32[2048]{0:T(1024)} %param.31, s32[]{:T(128)} %select_n.5), calls=%async_computation.16 | async-start | bytes 8704 | tf_op jit(solution)/shard_map/dynamic_slice | solution.py:53
  745.8 70.3 %dynamic-slice-start.2 = ((f32[2048]{0:T(1024)}, s32[]{:T(128)}), f32[1024]{0:T(1024)S(1)}, s32[]{:S(2)}) async-start(f32[2048]{0:T(1024)} %param.33, s32[]{:T(128)} %select_n.5), calls=%async_computation.17 | async-start | bytes 8704 | tf_op jit(solution)/shard_map/dynamic_slice | solution.py:54
  745.8 70.3 %copy-start.14 = (f32[2048]{0:T(1024)S(1)}, f32[2048]{0:T(1024)}, u32[]{:S(2)}) copy-start(f32[2048]{0:T(1024)} %param.35) | copy-start | bytes 24580
  821.7 7.3 copy-start
  821.7 20.9 %all-gather.24.cloned.1.call-start = ((), (), s32[]{:S(2)}) async-start(), calls=%async_computation.11 | async-start | bytes 2359296 | tf_op jit(solution)/shard_map/all_gather | solution.py:64
  831.3 13.2 %copy-start.16 = (f32[2048]{0:T(1024)S(1)}, f32[2048]{0:T(1024)}, u32[]{:S(2)}) copy-start(f32[2048]{0:T(1024)} %param.21) | copy-start | bytes 24580
  831.3 50.4 %reduce-scatter.8.cloned.1.call-start = ((), (), s32[]{:S(2)}) async-start(), calls=%async_computation.12 | async-start | bytes 2359296 | tf_op jit(solution)/shard_map/reduce_scatter | solution.py:70
  842.5 1.9 copy-start.6
  871.4 10.3 %copy-start.1 = (bf16[384,1024]{1,0:T(8,128)(2,1)S(1)}, bf16[384,1024]{1,0:T(8,128)(2,1)}, u32[]{:S(2)}) copy-start(bf16[384,1024]{1,0:T(8,128)(2,1)} %add_convert_fusion.1) | copy-start | bytes 2359300
Sparse Core Ops, SparseCore 0:
  8.9 12.5 all-gather.25
  23.6 177.2 all-gather.27
  203.1 174.2 all-gather.11
  379.5 174.2 all-gather.13
  570.6 7.1 reduce-scatter.3
  580.2 11.0 all-gather.15
  593.4 73.9 all-gather.17
  669.5 71.3 all-gather.19
  743.0 73.1 all-gather.21
  821.8 7.1 reduce-scatter.5
  831.4 11.0 all-gather.23
  871.5 10.1 reduce-scatter.7
